TPU v7x, 32 devices: a whole 2x2x4 slice. The times are simulated.
32 devices in a mesh: fs: 16 (over z, y, x), tp: 2 (over core).
Axes of the slice: x: 2, y: 2, z: 4, core: 2. Of those that a mesh axis runs over, the one named last changes fastest.
Arguments:
- tokens: bfloat16 [4096, 2048], P('fs'), may hold values from -6 to 6
- routes: int32 [4096, 6], P('fs'), may hold values from 0 to 15, all different within a row; in each aligned block of 256 rows (0 to 255, 256 to 511, ...) at most 160 rows name the same one
- route_weights: float32 [4096, 6], P('fs'), may hold values from 0.1 to 1
- norm_gain: float32 [2048], P('fs'), may hold values from 0.1 to 1.9
- expert_gate: float32 [16, 2048, 1024], P(None, 'fs', 'tp'), may hold values from -0.125 to 0.125
- expert_up: float32 [16, 2048, 1024], P(None, 'fs', 'tp'), may hold values from -0.125 to 0.125
- expert_down: float32 [16, 2048, 1024], P(None, 'fs', 'tp'), may hold values from -0.1875 to 0.1875
- shared_gate: float32 [2048, 1024], P('fs', 'tp'), may hold values from -0.125 to 0.125
- shared_up: float32 [2048, 1024], P('fs', 'tp'), may hold values from -0.125 to 0.125
- shared_down: float32 [2048, 1024], P('fs', 'tp'), may hold values from -0.1875 to 0.1875
Outputs:
- layer_output: bfloat16 [4096, 2048], P('fs', 'tp')
- sample_gate: bfloat16 [16, 2048, 1024], P('fs', None, 'tp')
- sample_up: bfloat16 [16, 2048, 1024], P('fs', None, 'tp')
- sample_down: bfloat16 [16, 2048, 1024], P('fs', None, 'tp')
- common_gate: bfloat16 [2048, 1024], P(None, 'tp')
- common_up: bfloat16 [2048, 1024], P(None, 'tp')
- common_down: bfloat16 [2048, 1024], P(None, 'tp')
Inputs may be any that keep to these rules, and one draw needn't show every extreme that they name: `routes`: each row names 6 different experts. In each aligned block of 256 rows (the rows of one index of fs) no expert is named by more than 160 rows, a bound that some expert reaches in some blocks.
All inputs are finite; a program needn't handle non-finite values.
Results may differ from a plain program's by a relative error of at most 0.015.
Values may be sent and summed in bfloat16 or wider, within the bound.
A program may use at most 128 MiB of HBM per device.

v0:
```python
import jax
import jax.numpy as jnp
from jax import lax
from jax.sharding import PartitionSpec as P

EPSILON = 1e-06


def normalize(tokens):
    values = tokens.astype(jnp.float32)
    scale = lax.rsqrt(jnp.mean(values * values, axis=-1, keepdims=True) + EPSILON)
    return (values * scale).astype(jnp.bfloat16)


def body(
    tokens,
    routes,
    route_weights,
    norm_gain,
    expert_gate,
    expert_up,
    expert_down,
    shared_gate,
    shared_up,
    shared_down,
):
    tp_count = lax.axis_size("tp")
    tp_index = lax.axis_index("tp")
    fs_count = lax.axis_size("fs")
    tok_rows, width = tokens.shape
    experts = expert_gate.shape[0]
    share = tok_rows // tp_count
    own_experts = experts // fs_count
    normed = normalize(tokens)
    own_normed = lax.dynamic_slice_in_dim(normed, tp_index * share, share, 0)
    own_routes = lax.dynamic_slice_in_dim(routes, tp_index * share, share, 0)
    own_weights = lax.dynamic_slice_in_dim(route_weights, tp_index * share, share, 0)
    member = own_routes[None, :, :] == jnp.arange(experts, dtype=jnp.int32)[:, None, None]
    dense = jnp.sum(jnp.where(member, own_weights[None, :, :], 0.0), axis=2)
    gathered = lax.all_gather(own_normed, "fs", axis=0, tiled=True)
    dense_all = lax.all_gather(dense, "fs", axis=0, tiled=False)
    gain_rows = norm_gain[None, :, None]
    rounded = (
        (expert_gate * gain_rows).astype(jnp.bfloat16),
        (expert_up * gain_rows).astype(jnp.bfloat16),
        expert_down.astype(jnp.bfloat16),
    )
    sample_gate, sample_up, sample_down = (
        lax.all_to_all(rounded[0], "fs", split_axis=0, concat_axis=1, tiled=True),
        lax.all_to_all(rounded[1], "fs", split_axis=0, concat_axis=1, tiled=True),
        lax.all_to_all(rounded[2], "fs", split_axis=0, concat_axis=1, tiled=True),
    )
    common_gate, common_up, common_down = (
        lax.all_gather(
            (shared_gate * norm_gain[:, None]).astype(jnp.bfloat16), "fs", axis=0, tiled=True
        ),
        lax.all_gather(
            (shared_up * norm_gain[:, None]).astype(jnp.bfloat16), "fs", axis=0, tiled=True
        ),
        lax.all_gather(shared_down.astype(jnp.bfloat16), "fs", axis=0, tiled=True),
    )
    shared_gate_act = jnp.dot(normed, common_gate, preferred_element_type=jnp.float32)
    shared_up_act = jnp.dot(normed, common_up, preferred_element_type=jnp.float32)
    shared_hidden = (jax.nn.silu(shared_gate_act) * shared_up_act).astype(jnp.bfloat16)
    shared_part = jnp.einsum(
        "th,dh->td", shared_hidden, common_down, preferred_element_type=jnp.float32
    ).astype(jnp.bfloat16)
    shared_parts = lax.all_to_all(
        shared_part.reshape(tok_rows, tp_count, width // tp_count).transpose(1, 0, 2),
        "tp",
        split_axis=0,
        concat_axis=0,
        tiled=True,
    )
    shared_sum = jnp.sum(shared_parts.astype(jnp.float32), axis=0)
    scale_all = lax.dynamic_slice_in_dim(
        dense_all, lax.axis_index("fs") * own_experts, own_experts, 1
    )
    total = None
    for expert in range(own_experts):
        scale = scale_all[:, expert, :].reshape(-1)[:, None]
        for shift in range(tp_count):
            gate_w, up_w, down_w = (sample_gate[expert], sample_up[expert], sample_down[expert])
            if shift:
                ring = [(i, (i + shift) % tp_count) for i in range(tp_count)]
                gate_w, up_w, down_w = (
                    lax.ppermute(gate_w, "tp", ring),
                    lax.ppermute(up_w, "tp", ring),
                    lax.ppermute(down_w, "tp", ring),
                )
            gate = jnp.dot(gathered, gate_w, preferred_element_type=jnp.float32)
            upward = jnp.dot(gathered, up_w, preferred_element_type=jnp.float32)
            hidden = (jax.nn.silu(gate) * upward * scale).astype(jnp.bfloat16)
            part = jnp.einsum("rf,df->rd", hidden, down_w, preferred_element_type=jnp.float32)
            total = part if total is None else total + part
    routed = lax.psum_scatter(total.astype(jnp.bfloat16), "fs", scatter_dimension=0, tiled=True)
    routed = lax.all_to_all(routed, "tp", split_axis=1, concat_axis=0, tiled=True)
    layer_output = (routed.astype(jnp.float32) + shared_sum).astype(jnp.bfloat16)
    return (layer_output, sample_gate, sample_up, sample_down, common_gate, common_up, common_down)


def solution(mesh):
    return jax.shard_map(
        body,
        mesh=mesh,
        in_specs=(
            P("fs", None),
            P("fs", None),
            P("fs", None),
            P("fs"),
            P(None, "fs", "tp"),
            P(None, "fs", "tp"),
            P(None, "fs", "tp"),
            P("fs", "tp"),
            P("fs", "tp"),
            P("fs", "tp"),
        ),
        out_specs=(
            P("fs", "tp"),
            P("fs", None, "tp"),
            P("fs", None, "tp"),
            P("fs", None, "tp"),
            P(None, "tp"),
            P(None, "tp"),
            P(None, "tp"),
        ),
        check_vma=False,
    )
```

profile of v0, /device:TPU:11, one launch (start us, length us, event | category | flops | bytes accessed | tf_op | source)
XLA Modules:
  0.0 607.8 jit_solution(15371878558450184911)
XLA Ops:
  11.1 6.8 %multiply_convert_fusion.2 = (bf16[16,128,512]{2,1,0:T(8,128)(2,1)}, bf16[16,128,512]{2,1,0:T(8,128)(2,1)}) fusion(f32[16,128,512]{2,1,0:T(8,128)} %param.15, f32[128]{0:T(128)S(1)} %copy-done.8, f32[16,128,512]{2,1,0:T(8,128)} %param.14), kind=kLoop, calls=%fused_computation.3 | loop fusion | flops 4194304 | bytes 12583424 | tf_op jit(solution)/shard_map/convert_element_type | solution.py:45
  17.9 6.8 %all-to-all-start = ((bf16[16,128,512]{2,1,0:T(8,128)(2,1)}), bf16[16,128,512]{2,1,0:T(8,128)(2,1)S(1)}, u32[]{:S(2)}, u32[]{:S(2)}) async-start(bf16[16,128,512]{2,1,0:T(8,128)(2,1)} %get-tuple-element.8), calls=%async_computation | async-start | bytes 4194304 | tf_op jit(solution)/shard_map/all_to_all | solution.py:49
  26.5 74.4 %all-to-all-done = bf16[16,128,512]{2,1,0:T(8,128)(2,1)S(1)} async-done(((bf16[16,128,512]{2,1,0:T(8,128)(2,1)}), bf16[16,128,512]{2,1,0:T(8,128)(2,1)S(1)}, u32[]{:S(2)}, u32[]{:S(2)}) %all-to-all-start) | async-done | bytes 2097184 | tf_op jit(solution)/shard_map/all_to_all | solution.py:49
  101.0 6.9 %all-to-all-start.1 = ((bf16[16,128,512]{2,1,0:T(8,128)(2,1)}), bf16[16,128,512]{2,1,0:T(8,128)(2,1)}, u32[]{:S(2)}, u32[]{:S(2)}) async-start(bf16[16,128,512]{2,1,0:T(8,128)(2,1)} %get-tuple-element.7), calls=%async_computation.1 | async-start | bytes 4194304 | tf_op jit(solution)/shard_map/all_to_all | solution.py:50
  108.6 3.9 convert_element_type.59
  112.5 81.0 %all-to-all-done.1 = bf16[16,128,512]{2,1,0:T(8,128)(2,1)} async-done(((bf16[16,128,512]{2,1,0:T(8,128)(2,1)}), bf16[16,128,512]{2,1,0:T(8,128)(2,1)}, u32[]{:S(2)}, u32[]{:S(2)}) %all-to-all-start.1) | async-done | bytes 2097184 | tf_op jit(solution)/shard_map/all_to_all | solution.py:50
  193.5 9.3 %all-to-all-start.2 = ((bf16[16,128,512]{2,1,0:T(8,128)(2,1)}), bf16[16,128,512]{2,1,0:T(8,128)(2,1)}, u32[]{:S(2)}, u32[]{:S(2)}) async-start(bf16[16,128,512]{2,1,0:T(8,128)(2,1)} %convert_element_type.59), calls=%async_computation.2 | async-start | bytes 4194304 | tf_op jit(solution)/shard_map/all_to_all | solution.py:51
  202.8 4.0 collective-permute-start
  207.7 68.8 %all-gather = f32[256,128]{1,0:T(8,128)S(1)} all-gather(f32[16,128]{1,0:T(8,128)S(1)} %select_reduce_fusion), channel_id=2, replica_groups=mesh['fs'=16,'tp'=2] {'fs'}, dimensions={0}, use_global_device_ids=true | all-gather | bytes 139264 | tf_op jit(solution)/shard_map/all_gather | solution.py:41
  276.5 8.9 %collective-permute-start.1 = (bf16[2048,512]{1,0:T(8,128)(2,1)}, bf16[2048,512]{1,0:T(8,128)(2,1)}, u32[]{:S(2)}, u32[]{:S(2)}) collective-permute-start(bf16[2048,512]{1,0:T(8,128)(2,1)} %bitcast.1), channel_id=1, source_target_pairs={{0,1},{1,0},{2,3},{3,2},{4,5},{5,4},{6,7},{7,6},{8,9},{9,8},{10,11... | collective-permute-start | bytes 6291464 | tf_op jit(solution)/shard_map/ppermute | solution.py:88
  285.5 9.8 %fusion.16 = f32[2048,512]{1,0:T(8,128)} fusion(bf16[2048,2048]{1,0:T(8,128)(2,1)} %all-gather.6.cloned.1.call-done, bf16[2048,512]{1,0:T(8,128)(2,1)S(1)} %bitcast.41), kind=kOutput, calls=%fused_computation.38 | convolution fusion | flops 4294967296 | bytes 14680064 | tf_op jit(solution)/shard_map/dot_general | solution.py:91
  295.3 7.6 %fusion.17 = f32[2048,512]{1,0:T(8,128)} fusion(bf16[2048,2048]{1,0:T(8,128)(2,1)S(1)} %copy-done.9, bf16[2048,512]{1,0:T(8,128)(2,1)} %collective-permute-done), kind=kOutput, calls=%fused_computation.39 | convolution fusion | flops 4294967296 | bytes 14680064 | tf_op jit(solution)/shard_map/dot_general | solution.py:91
  302.9 7.6 %fusion.18 = f32[2048,512]{1,0:T(8,128)} fusion(bf16[2048,2048]{1,0:T(8,128)(2,1)S(1)} %copy-done.9, bf16[2048,512]{1,0:T(8,128)(2,1)} %collective-permute-done.1), kind=kOutput, calls=%fused_computation.40 | convolution fusion | flops 4294967296 | bytes 14680064 | tf_op jit(solution)/shard_map/dot_general | solution.py:92
  310.5 16.6 %fusion.6 = f32[2048,2048]{1,0:T(8,128)} fusion(bf16[2048,512]{1,0:T(8,128)(2,1)} %bitcast.4, f32[2048,512]{1,0:T(8,128)} %fusion.16, bf16[2048,2048]{1,0:T(8,128)(2,1)} %all-gather.6.cloned.1.call-done, bf16[2048,512]{1,0:T(8,128)(2,1)} %bitcast.1, f32[2048]{0:T(1024)S(1)} %bitcast.48), kind=kOutput, calls=%fused_computation.18 | convolution fusion | flops 8597274624 | bytes 33562624 | tf_op jit(solution)/shard_map/rf,df->rd/dot_general | solution.py:94
  327.0 13.6 %add_convert_fusion = bf16[2048,2048]{1,0:T(8,128)(2,1)} fusion(f32[2048,2048]{1,0:T(8,128)} %fusion.6, bf16[2048,512]{1,0:T(8,128)(2,1)} %collective-permute-done.2, f32[2048,512]{1,0:T(8,128)} %fusion.18, f32[2048,512]{1,0:T(8,128)} %fusion.17, f32[2048]{0:T(1024)S(1)} %bitcast.49), kind=kOutput, calls=%fused_computation | convolution fusion | flops 4310695936 | bytes 35659776 | tf_op jit(solution)/shard_map/rf,df->rd/dot_general | solution.py:94
  340.7 3.1 fusion.19
  343.8 55.0 %all-gather.12.cloned.1.call-done = bf16[2048,512]{1,0:T(8,128)(2,1)} async-done(((bf16[128,512]{1,0:T(8,128)(2,1)}), bf16[2048,512]{1,0:T(8,128)(2,1)}) %all-gather.12.cloned.1.call-update) | async-done | bytes 2097168 | tf_op jit(solution)/shard_map/all_gather | solution.py:60
  398.8 4.7 convolution_convert_fusion
  403.5 2.3 copy.30
  405.7 5.2 all-to-all-start.4
  413.9 167.8 %reduce-scatter.2.cloned.1.call-done = bf16[128,2048]{1,0:T(8,128)(2,1)} async-done(((bf16[2048,2048]{1,0:T(8,128)(2,1)}), bf16[128,2048]{1,0:T(8,128)(2,1)}) %reduce-scatter.2.cloned.1.call-update) | async-done | bytes 524304 | tf_op jit(solution)/shard_map/reduce_scatter | solution.py:96
  582.8 4.7 all_to_all.54
  590.9 3.2 copy.39
  594.1 3.2 copy.40
  (56 shorter events, 18.9 us)
Async XLA Ops:
  7.2 200.4 %copy-start = (f32[256,6]{0,1:T(8,128)S(1)}, f32[256,6]{0,1:T(8,128)}, u32[]{:S(2)}) copy-start(f32[256,6]{0,1:T(8,128)} %param.12) | copy-start | bytes 18436
  7.2 3.9 copy-start.8
  7.2 278.3 %all-gather.6.cloned.1.call-start = ((), (), s32[]{:S(2)}) async-start(), calls=%async_computation.6 | async-start | bytes 8912896 | tf_op jit(solution)/shard_map/all_gather | solution.py:40
  17.9 6.8 %copy-start.6 = (f32[128,512]{1,0:T(8,128)S(1)}, f32[128,512]{1,0:T(8,128)}, u32[]{:S(2)}) copy-start(f32[128,512]{1,0:T(8,128)} %param.17) | copy-start | bytes 786436
  17.9 83.0 %all-to-all-start = ((bf16[16,128,512]{2,1,0:T(8,128)(2,1)}), bf16[16,128,512]{2,1,0:T(8,128)(2,1)S(1)}, u32[]{:S(2)}, u32[]{:S(2)}) async-start(bf16[16,128,512]{2,1,0:T(8,128)(2,1)} %get-tuple-element.8), calls=%async_computation | async-start | bytes 4194304 | tf_op jit(solution)/shard_map/all_to_all | solution.py:49
  24.7 316.0 %all-gather.8.cloned.1.call-start = ((), (), s32[]{:S(2)}) async-start(), calls=%async_computation.8 | async-start | bytes 2228224 | tf_op jit(solution)/shard_map/all_gather | solution.py:54
  101.0 92.5 %all-to-all-start.1 = ((bf16[16,128,512]{2,1,0:T(8,128)(2,1)}), bf16[16,128,512]{2,1,0:T(8,128)(2,1)}, u32[]{:S(2)}, u32[]{:S(2)}) async-start(bf16[16,128,512]{2,1,0:T(8,128)(2,1)} %get-tuple-element.7), calls=%async_computation.1 | async-start | bytes 4194304 | tf_op jit(solution)/shard_map/all_to_all | solution.py:50
  107.8 235.9 %all-gather.10.cloned.1.call-start = ((), (), s32[]{:S(2)}) async-start(), calls=%async_computation.9 | async-start | bytes 2228224 | tf_op jit(solution)/shard_map/all_gather | solution.py:57
  108.6 98.3 %copy-start.5 = (f32[128,512]{1,0:T(8,128)S(1)}, f32[128,512]{1,0:T(8,128)}, u32[]{:S(2)}) copy-start(f32[128,512]{1,0:T(8,128)} %param.19) | copy-start | bytes 786436
  108.6 99.1 %copy-start.7 = (s32[256,6]{0,1:T(8,128)S(1)}, s32[256,6]{0,1:T(8,128)}, u32[]{:S(2)}) copy-start(s32[256,6]{0,1:T(8,128)} %param.11) | copy-start | bytes 18436
  193.5 91.9 %all-to-all-start.2 = ((bf16[16,128,512]{2,1,0:T(8,128)(2,1)}), bf16[16,128,512]{2,1,0:T(8,128)(2,1)}, u32[]{:S(2)}, u32[]{:S(2)}) async-start(bf16[16,128,512]{2,1,0:T(8,128)(2,1)} %convert_element_type.59), calls=%async_computation.2 | async-start | bytes 4194304 | tf_op jit(solution)/shard_map/all_to_all | solution.py:51
  202.8 196.0 %all-gather.12.cloned.1.call-start = ((), (), s32[]{:S(2)}) async-start(), calls=%async_computation.10 | async-start | bytes 2228224 | tf_op jit(solution)/shard_map/all_gather | solution.py:60
  202.8 92.5 %collective-permute-start = (bf16[2048,512]{1,0:T(8,128)(2,1)S(1)}, bf16[2048,512]{1,0:T(8,128)(2,1)}, u32[]{:S(2)}, u32[]{:S(2)}) collective-permute-start(bf16[2048,512]{1,0:T(8,128)(2,1)S(1)} %bitcast.40), channel_id=1, source_target_pairs={{0,1},{1,0},{2,3},{3,2},{4,5},{5,4},{6,7},{7,6},{8,9},{9,8},{10,11... | collective-permute-start | bytes 6291464 | tf_op jit(solution)/shard_map/ppermute | solution.py:87
  207.5 374.1 %reduce-scatter.2.cloned.1.call-start = ((), (), s32[]{:S(2)}) async-start(), calls=%async_computation.7 | async-start | bytes 8912896 | tf_op jit(solution)/shard_map/reduce_scatter | solution.py:96
  276.5 26.4 %collective-permute-start.1 = (bf16[2048,512]{1,0:T(8,128)(2,1)}, bf16[2048,512]{1,0:T(8,128)(2,1)}, u32[]{:S(2)}, u32[]{:S(2)}) collective-permute-start(bf16[2048,512]{1,0:T(8,128)(2,1)} %bitcast.1), channel_id=1, source_target_pairs={{0,1},{1,0},{2,3},{3,2},{4,5},{5,4},{6,7},{7,6},{8,9},{9,8},{10,11... | collective-permute-start | bytes 6291464 | tf_op jit(solution)/shard_map/ppermute | solution.py:88
  285.4 41.6 %collective-permute-start.2 = (bf16[2048,512]{1,0:T(8,128)(2,1)}, bf16[2048,512]{1,0:T(8,128)(2,1)}, u32[]{:S(2)}, u32[]{:S(2)}) collective-permute-start(bf16[2048,512]{1,0:T(8,128)(2,1)} %bitcast.4), channel_id=1, source_target_pairs={{0,1},{1,0},{2,3},{3,2},{4,5},{5,4},{6,7},{7,6},{8,9},{9,8},{10,11... | collective-permute-start | bytes 6291464 | tf_op jit(solution)/shard_map/ppermute | solution.py:89
  285.5 9.8 %copy-start.9 = (bf16[2048,2048]{1,0:T(8,128)(2,1)S(1)}, bf16[2048,2048]{1,0:T(8,128)(2,1)}, u32[]{:S(2)}) copy-start(bf16[2048,2048]{1,0:T(8,128)(2,1)} %all-gather.6.cloned.1.call-done) | copy-start | bytes 25165828
  405.7 6.9 %all-to-all-start.4 = ((bf16[2,256,1024]{2,1,0:T(8,128)(2,1)}), bf16[2,256,1024]{2,1,0:T(8,128)(2,1)S(1)}, u32[]{:S(2)}, u32[]{:S(2)}) async-start(bf16[2,256,1024]{2,1,0:T(8,128)(2,1)} %bitcast.43), calls=%async_computation.5 | async-start | bytes 2097152 | tf_op jit(solution)/shard_map/all_to_all | solution.py:68
  590.9 6.4 %copy-start.2 = (bf16[2048,512]{1,0:T(8,128)(2,1)S(1)}, bf16[2048,512]{1,0:T(8,128)(2,1)}, u32[]{:S(2)}) copy-start(bf16[2048,512]{1,0:T(8,128)(2,1)} %all-gather.8.cloned.1.call-done) | copy-start | bytes 6291460
  594.1 4.5 copy-start.3
  597.3 2.6 copy-start.4
  597.3 4.0 copy-start.1
Sparse Core Ops, SparseCore 0:
  11.3 187.2 all-gather.5
  202.0 71.4 all-gather.7
  276.8 59.5 all-gather.9
  339.6 59.1 all-gather.11
  400.9 180.7 reduce-scatter.1
where the time goes:
time: 609 us; the launch traced here: 608 us
  waiting for transfers between devices  381 us (63%)
  blocking collectives  73.5 us (12%)
  matrix products  62.9 us (10%)
  starting transfers between devices  41.3 us (7%)
  other arithmetic  19.5 us (3%)
  local copies, waits for them, and re-layouts  15.9 us (3%)
  between operations  13.9 us (2%)
    reduce_scatter x1, waiting for transfers between devices, body(): lax.psum_scatter(total.astype(jnp.bfloat16), 'fs', scatter_dimension=0, t...  168 us
    all_to_all x1, waiting for transfers between devices, body(): lax.all_to_all(rounded[1], 'fs', split_axis=0, concat_axis=1, tiled=True)  81 us
    all_to_all x1, waiting for transfers between devices, body(): lax.all_to_all(rounded[0], 'fs', split_axis=0, concat_axis=1, tiled=True)  74.4 us
    all_gather x1, blocking collectives, body(): dense_all = lax.all_gather(dense, 'fs', axis=0, tiled=False)  68.8 us
    all_gather x1, waiting for transfers between devices, body(): lax.all_gather(shared_down.astype(jnp.bfloat16), 'fs', axis=0, tiled=True)  55 us
    dot_general x2, matrix products, body(): jnp.einsum('rf,df->rd', hidden, down_w, preferred_element_type=jnp.float32)  30.1 us
    dot_general x2, matrix products, body(): gate = jnp.dot(gathered, gate_w, preferred_element_type=jnp.float32)  17.4 us
  transfers between devices with their start and end apart: 12, of which 5 were waited for; matrix products, arithmetic and copies ran while one was open for 13% of the time, Pallas kernels for 0%

commit v1 on v0

--- a/solution.py
+++ b/solution.py
@@ -4,6 +4,18 @@
 from jax.sharding import PartitionSpec as P
 
 EPSILON = 1e-06
+
+
+def collect(shard, axis, dim):
+    ways, here, turn = (lax.axis_size(axis), lax.axis_index(axis), shard.shape[dim])
+    line, have = (shard, 1)
+    while have < ways:
+        line = jnp.concatenate(
+            [line, lax.ppermute(line, axis, [(d, (d - have) % ways) for d in range(ways)])],
+            axis=dim,
+        )
+        have = 2 * have
+    return jnp.roll(line, here * turn, axis=dim)
 
 
 def normalize(tokens):
@@ -57,7 +69,7 @@
         lax.all_gather(
             (shared_up * norm_gain[:, None]).astype(jnp.bfloat16), "fs", axis=0, tiled=True
         ),
-        lax.all_gather(shared_down.astype(jnp.bfloat16), "fs", axis=0, tiled=True),
+        collect(shared_down.astype(jnp.bfloat16), "fs", 0),
     )
     shared_gate_act = jnp.dot(normed, common_gate, preferred_element_type=jnp.float32)
     shared_up_act = jnp.dot(normed, common_up, preferred_element_type=jnp.float32)

time: 609 us -> 551 us (0.905)
  waiting for transfers between devices: 381 us -> 233 us
  blocking collectives: 73.5 us -> 164 us
  local copies, waits for them, and re-layouts: 15.9 us -> 28.4 us
  starting transfers between devices: 41.3 us -> 29.3 us
    reduce_scatter x1, waiting for transfers between devices: 168 us -> 81.3 us  [body(): lax.psum_scatter(total.astype(jnp.bfloat16), 'fs', scatter_dimension=0, t...]
    all_to_all x0 -> x1, blocking collectives: none -> 85.9 us  [body(): lax.all_to_all(rounded[0], 'fs', split_axis=0, concat_axis=1, tiled=True)]
    all_to_all x1 -> x0, waiting for transfers between devices: 74.4 us -> none  [body(): lax.all_to_all(rounded[0], 'fs', split_axis=0, concat_axis=1, tiled=True)]
    ppermute x0 -> x4, waiting for transfers between devices: none -> 67.9 us  [collect(): lax.ppermute(line, axis, [(d, (d - have) % ways) for d in range(ways)])]
    all_gather x1 -> x0, waiting for transfers between devices: 55 us -> none  [body(): lax.all_gather(shared_down.astype(jnp.bfloat16), 'fs', axis=0, tiled=True)]
    unnamed x26 -> x37, local copies, waits for them, and re-layouts: 11.7 us -> 18.7 us
    all_to_all x1 -> x0, starting transfers between devices: 6.77 us -> none  [body(): lax.all_to_all(rounded[0], 'fs', split_axis=0, concat_axis=1, tiled=True)]
  transfers between devices with their start and end apart: 12 -> 14, of which waited for: 5 -> 7; matrix products, arithmetic and copies ran while one was open for 13% -> 17% of each run, Pallas kernels for 0% -> 0%
where the time goes in v1:
time: 551 us
  waiting for transfers between devices  233 us (42%)
  blocking collectives  164 us (30%)
  matrix products  63.2 us (11%)
  starting transfers between devices  29.3 us (5%)
  local copies, waits for them, and re-layouts  28.4 us (5%)
  other arithmetic  18.9 us (3%)
  between operations  13.9 us (3%)
    all_to_all x1, blocking collectives, body(): lax.all_to_all(rounded[0], 'fs', split_axis=0, concat_axis=1, tiled=True)  85.9 us
    all_to_all x1, waiting for transfers between devices, body(): lax.all_to_all(rounded[1], 'fs', split_axis=0, concat_axis=1, tiled=True)  81.6 us
    reduce_scatter x1, waiting for transfers between devices, body(): lax.psum_scatter(total.astype(jnp.bfloat16), 'fs', scatter_dimension=0, t...  81.3 us
    all_gather x1, blocking collectives, body(): dense_all = lax.all_gather(dense, 'fs', axis=0, tiled=False)  72.2 us
    ppermute x4, waiting for transfers between devices, collect(): lax.ppermute(line, axis, [(d, (d - have) % ways) for d in range(ways)])  67.9 us
    dot_general x2, matrix products, body(): jnp.einsum('rf,df->rd', hidden, down_w, preferred_element_type=jnp.float32)  30.2 us
    unnamed x37, local copies, waits for them, and re-layouts  18.7 us
    dot_general x2, matrix products, body(): gate = jnp.dot(gathered, gate_w, preferred_element_type=jnp.float32)  17.3 us
  transfers between devices with their start and end apart: 14, of which 7 were waited for; matrix products, arithmetic and copies ran while one was open for 17% of the time, Pallas kernels for 0%

profile of v1, /device:TPU:11, one launch (start us, length us, event | category | flops | bytes accessed | tf_op | source)
XLA Modules:
  0.0 550.7 jit_solution(6024421141377645320)
XLA Ops:
  11.2 6.1 %multiply_convert_fusion.2 = (bf16[16,128,512]{2,1,0:T(8,128)(2,1)}, bf16[16,128,512]{2,1,0:T(8,128)(2,1)S(1)}) fusion(f32[16,128,512]{2,1,0:T(8,128)} %param.15, f32[128]{0:T(128)S(1)} %copy-done.10, f32[16,128,512]{2,1,0:T(8,128)} %param.14), kind=kLoop, calls=%fused_computation.3 | loop fusion | flops 4194304 | bytes 12583424 | tf_op jit(solution)/shard_map/convert_element_type | solution.py:57
  17.3 85.9 %all_to_all.54 = bf16[16,128,512]{2,1,0:T(8,128)(2,1)S(1)} all-to-all(bf16[16,128,512]{2,1,0:T(8,128)(2,1)S(1)} %get-tuple-element.10), channel_id=1, replica_groups=mesh['fs'=16,'tp'=2] {'fs'}, dimensions={0} | all-to-all | bytes 4194304 | tf_op jit(solution)/shard_map/all_to_all | solution.py:61
  103.2 5.0 all-to-all-start.1
  109.1 3.9 convert_element_type.59
  113.0 81.6 %all-to-all-done.1 = bf16[16,128,512]{2,1,0:T(8,128)(2,1)} async-done(((bf16[16,128,512]{2,1,0:T(8,128)(2,1)}), bf16[16,128,512]{2,1,0:T(8,128)(2,1)}, u32[]{:S(2)}, u32[]{:S(2)}) %all-to-all-start.1) | async-done | bytes 2097184 | tf_op jit(solution)/shard_map/all_to_all | solution.py:62
  194.6 7.4 %all-to-all-start.2 = ((bf16[16,128,512]{2,1,0:T(8,128)(2,1)}), bf16[16,128,512]{2,1,0:T(8,128)(2,1)}, u32[]{:S(2)}, u32[]{:S(2)}) async-start(bf16[16,128,512]{2,1,0:T(8,128)(2,1)} %convert_element_type.59), calls=%async_computation.2 | async-start | bytes 4194304 | tf_op jit(solution)/shard_map/all_to_all | solution.py:63
  203.2 72.2 %all-gather = f32[256,128]{1,0:T(8,128)S(1)} all-gather(f32[16,128]{1,0:T(8,128)S(1)} %select_reduce_fusion), channel_id=2, replica_groups=mesh['fs'=16,'tp'=2] {'fs'}, dimensions={0}, use_global_device_ids=true | all-gather | bytes 139264 | tf_op jit(solution)/shard_map/all_gather | solution.py:53
  275.5 7.0 %collective-permute-start.1 = (bf16[2048,512]{1,0:T(8,128)(2,1)}, bf16[2048,512]{1,0:T(8,128)(2,1)}, u32[]{:S(2)}, u32[]{:S(2)}) collective-permute-start(bf16[2048,512]{1,0:T(8,128)(2,1)} %bitcast.1), channel_id=1, source_target_pairs={{0,1},{1,0},{2,3},{3,2},{4,5},{5,4},{6,7},{7,6},{8,9},{9,8},{10,11... | collective-permute-start | bytes 6291464 | tf_op jit(solution)/shard_map/ppermute | solution.py:100
  282.6 9.7 %fusion.16 = f32[2048,512]{1,0:T(8,128)} fusion(bf16[2048,2048]{1,0:T(8,128)(2,1)} %all-gather.5.cloned.1.call-done, bf16[2048,512]{1,0:T(8,128)(2,1)S(1)} %bitcast.41), kind=kOutput, calls=%fused_computation.52 | convolution fusion | flops 4294967296 | bytes 14680064 | tf_op jit(solution)/shard_map/dot_general | solution.py:103
  292.3 7.6 %fusion.17 = f32[2048,512]{1,0:T(8,128)} fusion(bf16[2048,2048]{1,0:T(8,128)(2,1)S(1)} %copy-done.11, bf16[2048,512]{1,0:T(8,128)(2,1)} %collective-permute-done), kind=kOutput, calls=%fused_computation.53 | convolution fusion | flops 4294967296 | bytes 14680064 | tf_op jit(solution)/shard_map/dot_general | solution.py:103
  299.9 7.6 %fusion.18 = f32[2048,512]{1,0:T(8,128)} fusion(bf16[2048,2048]{1,0:T(8,128)(2,1)S(1)} %copy-done.11, bf16[2048,512]{1,0:T(8,128)(2,1)} %collective-permute-done.1), kind=kOutput, calls=%fused_computation.54 | convolution fusion | flops 4294967296 | bytes 14680064 | tf_op jit(solution)/shard_map/dot_general | solution.py:104
  307.5 16.6 %fusion.6 = f32[2048,2048]{1,0:T(8,128)} fusion(bf16[2048,512]{1,0:T(8,128)(2,1)} %bitcast.4, f32[2048,512]{1,0:T(8,128)} %fusion.16, bf16[2048,2048]{1,0:T(8,128)(2,1)} %all-gather.5.cloned.1.call-done, bf16[2048,512]{1,0:T(8,128)(2,1)} %bitcast.1, f32[2048]{0:T(1024)S(1)} %bitcast.48), kind=kOutput, calls=%fused_computation.19 | convolution fusion | flops 8597274624 | bytes 33562624 | tf_op jit(solution)/shard_map/rf,df->rd/dot_general | solution.py:106
  324.1 13.6 %add_convert_fusion = bf16[2048,2048]{1,0:T(8,128)(2,1)} fusion(f32[2048,2048]{1,0:T(8,128)} %fusion.6, bf16[2048,512]{1,0:T(8,128)(2,1)} %collective-permute-done.2, f32[2048,512]{1,0:T(8,128)} %fusion.18, f32[2048,512]{1,0:T(8,128)} %fusion.17, f32[2048]{0:T(1024)S(1)} %bitcast.49), kind=kOutput, calls=%fused_computation | convolution fusion | flops 4310695936 | bytes 35659776 | tf_op jit(solution)/shard_map/rf,df->rd/dot_general | solution.py:106
  340.5 4.3 collective-permute-done.3
  346.4 9.9 %collective-permute-done.4 = bf16[256,512]{1,0:T(8,128)(2,1)S(1)} collective-permute-done((bf16[256,512]{1,0:T(8,128)(2,1)S(1)}, bf16[256,512]{1,0:T(8,128)(2,1)S(1)}, u32[]{:S(2)}, u32[]{:S(2)}) %collective-permute-start.4) | collective-permute-done | bytes 262176 | tf_op jit(solution)/shard_map/ppermute | solution.py:14
  356.6 10.8 %collective-permute-done.5 = bf16[512,512]{1,0:T(8,128)(2,1)S(1)} collective-permute-done((bf16[512,512]{1,0:T(8,128)(2,1)S(1)}, bf16[512,512]{1,0:T(8,128)(2,1)S(1)}, u32[]{:S(2)}, u32[]{:S(2)}) %collective-permute-start.5) | collective-permute-done | bytes 524320 | tf_op jit(solution)/shard_map/ppermute | solution.py:14
  371.5 43.0 %collective-permute-done.6 = bf16[1024,512]{1,0:T(8,128)(2,1)} collective-permute-done((bf16[1024,512]{1,0:T(8,128)(2,1)}, bf16[1024,512]{1,0:T(8,128)(2,1)}, u32[]{:S(2)}, u32[]{:S(2)}) %collective-permute-start.6) | collective-permute-done | bytes 1048608 | tf_op jit(solution)/shard_map/ppermute | solution.py:14
  425.0 3.4 fusion.19
  428.5 4.8 convolution_convert_fusion
  435.5 4.5 all-to-all-start.4
  443.0 81.3 %reduce-scatter.2.cloned.1.call-done = bf16[128,2048]{1,0:T(8,128)(2,1)} async-done(((bf16[2048,2048]{1,0:T(8,128)(2,1)}), bf16[128,2048]{1,0:T(8,128)(2,1)}) %reduce-scatter.2.cloned.1.call-update) | async-done | bytes 524304 | tf_op jit(solution)/shard_map/reduce_scatter | solution.py:108
  525.3 6.3 %all_to_all.55 = bf16[128,2,1024]{2,0,1:T(8,128)(2,1)S(1)} all-to-all(bf16[128,2,1024]{2,0,1:T(8,128)(2,1)S(1)} %bitcast.44), channel_id=1, replica_groups=mesh['fs'=16,'tp'=2] {'tp'}, dimensions={1} | all-to-all | bytes 1048576 | tf_op jit(solution)/shard_map/all_to_all | solution.py:109
  535.1 3.2 copy.47
  538.3 3.2 copy.48
  (76 shorter events, 38.0 us)
Async XLA Ops:
  7.2 196.0 %copy-start = (f32[256,6]{0,1:T(8,128)S(1)}, f32[256,6]{0,1:T(8,128)}, u32[]{:S(2)}) copy-start(f32[256,6]{0,1:T(8,128)} %param.12) | copy-start | bytes 18436
  7.2 275.4 %all-gather.5.cloned.1.call-start = ((), (), s32[]{:S(2)}) async-start(), calls=%async_computation.6 | async-start | bytes 8912896 | tf_op jit(solution)/shard_map/all_gather | solution.py:52
  10.2 7.1 %copy-start.2 = (bf16[256,2048]{1,0:T(8,128)(2,1)}, bf16[256,2048]{1,0:T(8,128)(2,1)S(1)}, u32[]{:S(2)}) copy-start(bf16[256,2048]{1,0:T(8,128)(2,1)S(1)} %fusion.1) | copy-start | bytes 3145732
  17.3 90.9 %copy-start.7 = (f32[128,512]{1,0:T(8,128)S(1)}, f32[128,512]{1,0:T(8,128)}, u32[]{:S(2)}) copy-start(f32[128,512]{1,0:T(8,128)} %param.17) | copy-start | bytes 786436
  17.3 90.9 %copy-start.8 = (f32[128,512]{1,0:T(8,128)S(1)}, f32[128,512]{1,0:T(8,128)}, u32[]{:S(2)}) copy-start(f32[128,512]{1,0:T(8,128)} %param.18) | copy-start | bytes 786436
  103.2 91.4 %all-to-all-start.1 = ((bf16[16,128,512]{2,1,0:T(8,128)(2,1)}), bf16[16,128,512]{2,1,0:T(8,128)(2,1)}, u32[]{:S(2)}, u32[]{:S(2)}) async-start(bf16[16,128,512]{2,1,0:T(8,128)(2,1)} %get-tuple-element.9), calls=%async_computation.1 | async-start | bytes 4194304 | tf_op jit(solution)/shard_map/all_to_all | solution.py:62
  108.2 316.8 %all-gather.7.cloned.1.call-start = ((), (), s32[]{:S(2)}) async-start(), calls=%async_computation.8 | async-start | bytes 2228224 | tf_op jit(solution)/shard_map/all_gather | solution.py:66
  109.1 94.1 %copy-start.9 = (s32[256,6]{0,1:T(8,128)S(1)}, s32[256,6]{0,1:T(8,128)}, u32[]{:S(2)}) copy-start(s32[256,6]{0,1:T(8,128)} %param.11) | copy-start | bytes 18436
  194.6 87.9 %all-to-all-start.2 = ((bf16[16,128,512]{2,1,0:T(8,128)(2,1)}), bf16[16,128,512]{2,1,0:T(8,128)(2,1)}, u32[]{:S(2)}, u32[]{:S(2)}) async-start(bf16[16,128,512]{2,1,0:T(8,128)(2,1)} %convert_element_type.59), calls=%async_computation.2 | async-start | bytes 4194304 | tf_op jit(solution)/shard_map/all_to_all | solution.py:63
  201.9 226.5 %all-gather.9.cloned.1.call-start = ((), (), s32[]{:S(2)}) async-start(), calls=%async_computation.9 | async-start | bytes 2228224 | tf_op jit(solution)/shard_map/all_gather | solution.py:69
  202.0 90.3 %collective-permute-start = (bf16[2048,512]{1,0:T(8,128)(2,1)S(1)}, bf16[2048,512]{1,0:T(8,128)(2,1)}, u32[]{:S(2)}, u32[]{:S(2)}) collective-permute-start(bf16[2048,512]{1,0:T(8,128)(2,1)S(1)} %bitcast.40), channel_id=1, source_target_pairs={{0,1},{1,0},{2,3},{3,2},{4,5},{5,4},{6,7},{7,6},{8,9},{9,8},{10,11... | collective-permute-start | bytes 6291464 | tf_op jit(solution)/shard_map/ppermute | solution.py:99
  203.1 321.1 %reduce-scatter.2.cloned.1.call-start = ((), (), s32[]{:S(2)}) async-start(), calls=%async_computation.7 | async-start | bytes 8912896 | tf_op jit(solution)/shard_map/reduce_scatter | solution.py:108
  275.5 24.4 %collective-permute-start.1 = (bf16[2048,512]{1,0:T(8,128)(2,1)}, bf16[2048,512]{1,0:T(8,128)(2,1)}, u32[]{:S(2)}, u32[]{:S(2)}) collective-permute-start(bf16[2048,512]{1,0:T(8,128)(2,1)} %bitcast.1), channel_id=1, source_target_pairs={{0,1},{1,0},{2,3},{3,2},{4,5},{5,4},{6,7},{7,6},{8,9},{9,8},{10,11... | collective-permute-start | bytes 6291464 | tf_op jit(solution)/shard_map/ppermute | solution.py:100
  282.5 41.6 %collective-permute-start.2 = (bf16[2048,512]{1,0:T(8,128)(2,1)}, bf16[2048,512]{1,0:T(8,128)(2,1)}, u32[]{:S(2)}, u32[]{:S(2)}) collective-permute-start(bf16[2048,512]{1,0:T(8,128)(2,1)} %bitcast.4), channel_id=1, source_target_pairs={{0,1},{1,0},{2,3},{3,2},{4,5},{5,4},{6,7},{7,6},{8,9},{9,8},{10,11... | collective-permute-start | bytes 6291464 | tf_op jit(solution)/shard_map/ppermute | solution.py:101
  282.6 9.7 %copy-start.11 = (bf16[2048,2048]{1,0:T(8,128)(2,1)S(1)}, bf16[2048,2048]{1,0:T(8,128)(2,1)}, u32[]{:S(2)}) copy-start(bf16[2048,2048]{1,0:T(8,128)(2,1)} %all-gather.5.cloned.1.call-done) | copy-start | bytes 25165828
  339.3 5.6 %collective-permute-start.3 = (bf16[128,512]{1,0:T(8,128)(2,1)S(1)}, bf16[128,512]{1,0:T(8,128)(2,1)S(1)}, u32[]{:S(2)}, u32[]{:S(2)}) collective-permute-start(bf16[128,512]{1,0:T(8,128)(2,1)S(1)} %get-tuple-element.8), channel_id=1, source_target_pairs={{0,30},{2,0},{4,2},{6,4},{8,6},{10,8},{12,10},{14,12},{16,14},{18,... | collective-permute-start | bytes 393224 | tf_op jit(solution)/shard_map/ppermute | solution.py:14
  344.9 11.4 %collective-permute-start.4 = (bf16[256,512]{1,0:T(8,128)(2,1)S(1)}, bf16[256,512]{1,0:T(8,128)(2,1)S(1)}, u32[]{:S(2)}, u32[]{:S(2)}) collective-permute-start(bf16[256,512]{1,0:T(8,128)(2,1)S(1)} %pad_maximum_fusion.2), channel_id=1, source_target_pairs={{0,28},{2,30},{4,0},{6,2},{8,4},{10,6},{12,8},{14,10},{16,12},{18,... | collective-permute-start | bytes 786440 | tf_op jit(solution)/shard_map/ppermute | solution.py:14
  356.3 11.1 %collective-permute-start.5 = (bf16[512,512]{1,0:T(8,128)(2,1)S(1)}, bf16[512,512]{1,0:T(8,128)(2,1)S(1)}, u32[]{:S(2)}, u32[]{:S(2)}) collective-permute-start(bf16[512,512]{1,0:T(8,128)(2,1)S(1)} %pad_maximum_fusion.1), channel_id=1, source_target_pairs={{0,24},{2,26},{4,28},{6,30},{8,0},{10,2},{12,4},{14,6},{16,8},{18,... | collective-permute-start | bytes 1572872 | tf_op jit(solution)/shard_map/ppermute | solution.py:14
  368.4 46.0 %collective-permute-start.6 = (bf16[1024,512]{1,0:T(8,128)(2,1)}, bf16[1024,512]{1,0:T(8,128)(2,1)}, u32[]{:S(2)}, u32[]{:S(2)}) collective-permute-start(bf16[1024,512]{1,0:T(8,128)(2,1)} %pad_maximum_fusion), channel_id=1, source_target_pairs={{0,16},{2,18},{4,20},{6,22},{8,24},{10,26},{12,28},{14,30},{16,0},... | collective-permute-start | bytes 3145736 | tf_op jit(solution)/shard_map/ppermute | solution.py:14
  421.9 6.6 %copy-start.3 = (bf16[256,2048]{1,0:T(8,128)(2,1)S(1)}, bf16[256,2048]{1,0:T(8,128)(2,1)}, u32[]{:S(2)}) copy-start(bf16[256,2048]{1,0:T(8,128)(2,1)} %copy-done.2) | copy-start | bytes 3145732
  435.5 6.3 %all-to-all-start.4 = ((bf16[2,256,1024]{2,1,0:T(8,128)(2,1)}), bf16[2,256,1024]{2,1,0:T(8,128)(2,1)S(1)}, u32[]{:S(2)}, u32[]{:S(2)}) async-start(bf16[2,256,1024]{2,1,0:T(8,128)(2,1)} %bitcast.43), calls=%async_computation.5 | async-start | bytes 2097152 | tf_op jit(solution)/shard_map/all_to_all | solution.py:80
  535.1 6.4 %copy-start.4 = (bf16[2048,512]{1,0:T(8,128)(2,1)S(1)}, bf16[2048,512]{1,0:T(8,128)(2,1)}, u32[]{:S(2)}) copy-start(bf16[2048,512]{1,0:T(8,128)(2,1)} %all-gather.7.cloned.1.call-done) | copy-start | bytes 6291460
  538.3 4.5 copy-start.5
  538.3 5.8 %copy-start.1 = (f32[256,6]{0,1:T(8,128)S(1)}, f32[256,6]{0,1:T(8,128)}, u32[]{:S(2)}) copy-start(f32[256,6]{0,1:T(8,128)} %param.12) | copy-start | bytes 18436
  (2 other events, 5.0 us)
Sparse Core Ops, SparseCore 0:
  11.3 181.1 all-gather.4
  195.9 80.8 all-gather.6
  280.2 59.4 all-gather.8
  341.9 182.3 reduce-scatter.1
